TPU v7x, 1024 devices: a whole 8x8x8 slice. The times are simulated.
1024 devices in a mesh: dp: 8 (over x), kv: 64 (over z, y), tp: 2 (over core).
Axes of the slice: x: 8, y: 8, z: 8, core: 2. Of those that a mesh axis runs over, the one named last changes fastest.
Arguments:
- piece_tokens: bfloat16 [8192, 2048], P(('dp', 'kv')), parts along dimension 0, may hold values from -6 to 6
- dec_tokens: bfloat16 [6144, 4, 2048], P(('dp', 'kv')), parts along dimension 0, may hold values from -6 to 6
- norm_gain: float32 [2048], replicated, may hold values from 0.1 to 1.9
- query_weight: bfloat16 [2048, 1024], P(None, 'tp'), may hold values from -0.375 to 0.375
- key_weight: bfloat16 [2048, 256], P(None, 'tp'), may hold values from -0.125 to 0.125
- value_weight: bfloat16 [2048, 256], P(None, 'tp'), may hold values from -0.125 to 0.125
- gate_weight: bfloat16 [2048, 8], P(None, 'tp'), may hold values from -0.125 to 0.125
- gate_bias: float32 [8], P('tp'), may hold values from 3.4 to 11
- out_weight: bfloat16 [1024, 2048], P('tp'), may hold values from -0.1875 to 0.1875
- out_gain: float32 [2048], replicated, may hold values from 0.1 to 1.9
- past_keys: bfloat16 [131072, 2, 128], P(('dp', 'kv'), 'tp'), parts along dimension 0, may hold values from -41 to 41
- past_values: bfloat16 [131072, 2, 128], P(('dp', 'kv'), 'tp'), parts along dimension 0, may hold values from -6 to 6
- past_gate: float32 [8, 131072], P('tp', ('dp', 'kv')), parts along dimension 1, may hold values from -16384 to 0
- dec_keys: bfloat16 [6144, 512, 2, 128], P(('dp', 'kv'), None, 'tp'), parts along dimension 0, may hold values from -41 to 41
- dec_values: bfloat16 [6144, 512, 2, 128], P(('dp', 'kv'), None, 'tp'), parts along dimension 0, may hold values from -6 to 6
- dec_gate: float32 [6144, 8, 512], P(('dp', 'kv'), 'tp'), parts along dimension 0, may hold values from -512 to 0
- dec_lengths: int32 [6144], P(('dp', 'kv')), parts along dimension 0, may hold values from 1 to 512, as said below
Outputs:
- piece_out: bfloat16 [8192, 2048], P(('dp', 'kv')), parts along dimension 0
- dec_out: bfloat16 [6144, 4, 2048], P(('dp', 'kv')), parts along dimension 0
There are 8 independent parts, one for each index of `dp`. A program takes and returns all parts, laid end to end along the dimension named above; an argument that names none is the same for every part. Nothing has to cross between parts.
Inputs may be any that keep to these rules, and one draw needn't show every extreme that they name: `dec_lengths`: some decoding sequence has all 512 slots live in every draw.
All inputs are finite; a program needn't handle non-finite values.
Results may differ from a plain program's by a relative error of at most 0.015.
Values may be sent and summed in bfloat16 or wider, within the bound.
No kernel may reach another device: no remote copies, remote signals or barrier semaphores. Data moves between devices by JAX's collectives and lax.ppermute only.
A program may use at most 64 MiB of HBM per device.

v0:
```python
import functools

import jax
import jax.numpy as jnp
from jax import lax
from jax.experimental import pallas as pl
from jax.experimental.pallas import tpu as pltpu
from jax.sharding import Mesh
from jax.sharding import PartitionSpec as P

PART = ("z", "y", "tp")
DP_KV = ("dp", "z", "y")
FAR = 4
EPS = 1e-06
LANES = 128
F32 = jnp.float32
BF16 = jnp.bfloat16
ROOM = 20 * 1024 * 1024


def rms_scale(source, scale_gain):
    widened = source.astype(F32)
    return (
        widened * lax.rsqrt(jnp.mean(widened * widened, axis=-1, keepdims=True) + EPS) * scale_gain
    )


def three_parts(x):
    high = x.astype(BF16).astype(F32)
    rest = x - high
    middle = rest.astype(BF16).astype(F32)
    low = (rest - middle).astype(BF16).astype(F32)
    return high, middle, low


def lane_index(shape):
    return lax.broadcasted_iota(jnp.int32, shape, len(shape) - 1)


def row_index(shape):
    return lax.broadcasted_iota(jnp.int32, shape, 0)


def pack_lanes(x, heads):
    high, middle, low = three_parts(x)
    lane = lane_index(x.shape)
    middle = pltpu.roll(middle, heads, 1)
    low = pltpu.roll(low, 2 * heads, 1)
    return jnp.where(
        lane < heads,
        high,
        jnp.where(lane < 2 * heads, middle, jnp.where(lane < 3 * heads, low, 0.0)),
    )


def unpack_lanes(x, heads):
    return x + pltpu.roll(x, LANES - heads, 1) + pltpu.roll(x, LANES - 2 * heads, 1)


def proj_kernel(
    heads,
    tok_hbm,
    gain_ref,
    wq_hbm,
    wk_hbm,
    wv_hbm,
    wg_ref,
    bias_ref,
    share_ref,
    new_ref,
    tok_ref,
    wq_ref,
    wk_ref,
    wv_ref,
    sems,
):
    model, width = wq_ref.shape
    pieces = sems.shape[0] - 3
    depth = model // pieces
    moves = [(tok_hbm, tok_ref)]
    moves += [
        (wq_hbm.at[pl.ds(n * depth, depth)], wq_ref.at[pl.ds(n * depth, depth)])
        for n in range(pieces)
    ]
    moves += [(wk_hbm, wk_ref), (wv_hbm, wv_ref)]
    copies = [pltpu.make_async_copy(src, dst, sems.at[n]) for n, (src, dst) in enumerate(moves)]
    for copy in copies:
        copy.start()
    copies[0].wait()
    normed = rms_scale(tok_ref[...], gain_ref[...]).astype(BF16)
    rows = normed.shape[0]
    logits = dot_t(normed, wg_ref[...]) + bias_ref[...]
    gates = jnp.minimum(logits, 0.0) - jnp.log1p(jnp.exp(-jnp.abs(logits)))
    lane = lane_index((rows, LANES))
    run = jnp.zeros((rows, LANES), F32)
    for h in range(heads):
        run = jnp.where(lane == h, gates[:, h : h + 1], run)
    row = row_index((rows, LANES))
    step = 1
    while step < rows:
        run = run + jnp.where(row >= step, pltpu.roll(run, step, 0), 0.0)
        step *= 2
    packed = pack_lanes(run, heads).astype(BF16)
    queries = jnp.zeros((rows, width), F32)
    for n in range(pieces):
        copies[1 + n].wait()
        queries = queries + jnp.dot(
            normed[:, n * depth : (n + 1) * depth],
            wq_ref[n * depth : (n + 1) * depth, :],
            preferred_element_type=F32,
        )
    queries = queries.astype(BF16)
    for slot in range(share_ref.shape[0]):
        share_ref[slot, :, 0:width] = queries
        share_ref[slot, :, width:] = packed
    copies[1 + pieces].wait()
    new_ref[0:rows, :] = jnp.dot(normed, wk_ref[...], preferred_element_type=F32).astype(BF16)
    copies[2 + pieces].wait()
    new_ref[rows : 2 * rows, :] = jnp.dot(
        normed, wv_ref[...], preferred_element_type=F32
    ).astype(BF16)
    new_ref[2 * rows :, :] = packed


def piece_projections(tokens, gain, wq, wk, wv, wg, bias, near):
    rows, model = tokens.shape
    heads = bias.shape[0]
    width, head_dim = wq.shape[1], wk.shape[1]
    hbm = pl.BlockSpec(memory_space=pl.ANY)
    vmem = pl.BlockSpec(memory_space=pltpu.VMEM)
    return pl.pallas_call(
        functools.partial(proj_kernel, heads),
        out_shape=(
            jax.ShapeDtypeStruct((near, rows, width + LANES), BF16),
            jax.ShapeDtypeStruct((3 * rows, head_dim), BF16),
        ),
        in_specs=[hbm, vmem, hbm, hbm, hbm, vmem, vmem],
        out_specs=(vmem, vmem),
        scratch_shapes=[
            pltpu.VMEM((rows, model), BF16),
            pltpu.VMEM((model, width), BF16),
            pltpu.VMEM((model, head_dim), BF16),
            pltpu.VMEM((model, head_dim), BF16),
            pltpu.SemaphoreType.DMA((7,)),
        ],
        cost_estimate=cost(3.0, 3 << 20),
        name="piece_proj",
    )(
        tokens,
        gain.reshape(1, model),
        wq,
        wk,
        wv,
        wg.T,
        bias.reshape(1, heads),
    )


def pack_kernel(heads, pk_hbm, pv_hbm, gate_ref, past_ref, parts_ref, sems):
    count = pk_hbm.shape[0]
    moves = [(pk_hbm, past_ref.at[pl.ds(0, count)]), (pv_hbm, past_ref.at[pl.ds(count, count)])]
    copies = [pltpu.make_async_copy(src, dst, sems.at[n]) for n, (src, dst) in enumerate(moves)]
    for copy in copies:
        copy.start()
    halves = count // LANES
    block = heads * halves
    parts_ref[...] = jnp.zeros_like(parts_ref)
    for n, part in enumerate(three_parts(gate_ref[...])):
        for half in range(halves):
            at = n * block + half * heads
            parts_ref[at : at + heads, :] = part[:, half * LANES : (half + 1) * LANES]
    past_ref[2 * count :, :] = parts_ref[...].astype(BF16)
    for copy in copies:
        copy.wait()


def packed_past(past_keys, past_values, past_gate):
    count, head_dim = past_keys.shape
    heads = past_gate.shape[0]
    gate_rows = -(-3 * heads * (count // LANES) // 16) * 16
    hbm = pl.BlockSpec(memory_space=pl.ANY)
    vmem = pl.BlockSpec(memory_space=pltpu.VMEM)
    return pl.pallas_call(
        functools.partial(pack_kernel, heads),
        out_shape=jax.ShapeDtypeStruct((2 * count + gate_rows, head_dim), BF16),
        in_specs=[hbm, hbm, vmem],
        out_specs=vmem,
        scratch_shapes=[pltpu.VMEM((gate_rows, LANES), F32), pltpu.SemaphoreType.DMA((2,))],
        compiler_params=room(),
        cost_estimate=cost(2.0, 1 << 18),
        name="pack_past",
    )(past_keys, past_values, past_gate)


def room():
    return pltpu.CompilerParams(vmem_limit_bytes=ROOM)


def cost(micros, moved):
    return pl.CostEstimate(
        flops=int(micros * 15e6), bytes_accessed=int(moved), transcendentals=0
    )


def run_kernel(shared_ref, new_ref, past_ref, out_ref):
    near, rows = shared_ref.shape[0], shared_ref.shape[1]
    width = shared_ref.shape[2] - LANES
    totals = jnp.concatenate(
        [shared_ref[i, :, width:].astype(F32)[rows - 1 : rows, :] for i in range(near)], axis=0
    )
    run = new_ref[2 * rows :, :].astype(F32)
    run = jnp.where(lane_index(run.shape) < 16, run, pltpu.roll(totals, 16, 1)).astype(BF16)
    for slot in range(out_ref.shape[0]):
        out_ref[slot, 0 : 2 * rows, :] = new_ref[0 : 2 * rows, :]
        out_ref[slot, 2 * rows : 3 * rows, :] = run
        out_ref[slot, 3 * rows :, :] = past_ref[...]


def run_payload(shared, new_rows, past, far):
    near, rows, _ = shared.shape
    assert near == rows
    vmem = pl.BlockSpec(memory_space=pltpu.VMEM)
    return pl.pallas_call(
        run_kernel,
        out_shape=jax.ShapeDtypeStruct((far, 3 * rows + past.shape[0], LANES), BF16),
        in_specs=[vmem, vmem, vmem],
        out_specs=vmem,
        compiler_params=room(),
        cost_estimate=cost(1.0, 1 << 18),
        name="run_payload",
    )(shared, new_rows, past)


def dot_t(a, b):
    return lax.dot_general(a, b, (((1,), (1,)), ((), ())), preferred_element_type=F32)


def past_count(payload_rows, heads):
    count = LANES
    while 2 * count + -(-3 * heads * (count // LANES) // 16) * 16 < payload_rows:
        count += LANES
    return count


def attend_kernel(heads, sizes, place_ref, shared_ref, new_ref, out_ref):
    near, rows = shared_ref.shape[0], shared_ref.shape[1]
    far, head_dim = new_ref.shape[0], new_ref.shape[2]
    scale = head_dim ** (-0.5)
    width = heads * head_dim
    my_far, my_near = place_ref[0], place_ref[1]
    across, core = sizes[1] // far, place_ref[2]

    def block_place(block, alike):
        by_z = block * near + alike
        by_y = (alike // across) * sizes[1] + block * across + alike % across
        return jnp.where(core == 0, by_z, by_y)

    folded = [
        unpack_lanes(new_ref[f, 2 * rows : 3 * rows, :].astype(F32), heads) for f in range(far)
    ]
    totals = pltpu.roll(jnp.concatenate(folded, axis=0), LANES - 16, 1)
    shape = (8 + near, far * near)
    row = row_index(shape)
    wanted = jnp.where(row < 8, block_place(row, my_near), block_place(my_far, row - 8))
    source = lane_index(shape)
    earlier = (block_place(source // near, source % near) < wanted).astype(F32)
    before = jnp.dot(
        earlier, totals, preferred_element_type=F32, precision=lax.Precision.HIGHEST
    )
    new_count = far * rows
    key_run = jnp.concatenate(
        [folded[f] + before[f : f + 1, :] for f in range(far)]
        + [jnp.zeros((LANES - new_count, LANES), F32)],
        axis=0,
    )
    key_run = jnp.transpose(key_run)
    local = unpack_lanes(
        shared_ref[:, :, width:].reshape(near * rows, LANES).astype(F32), heads
    )
    row_run = jnp.concatenate(
        [local[i * rows : (i + 1) * rows, :] + before[8 + i : 9 + i, :] for i in range(near)],
        axis=0,
    )
    shape = (near * rows, LANES)
    row = row_index(shape)
    row_place = block_place(my_far, row // rows) * rows + row % rows
    lane = lane_index(shape)
    key_place = block_place(lane // rows, my_near) * rows + lane % rows
    visible = (key_place <= row_place) & (lane < new_count)
    new_keys = jnp.concatenate(
        [new_ref[f, 0:rows, :] for f in range(far)]
        + [jnp.zeros((LANES - new_count, head_dim), BF16)],
        axis=0,
    )
    new_values = jnp.concatenate(
        [new_ref[f, rows : 2 * rows, :] for f in range(far)]
        + [jnp.zeros((LANES - new_count, head_dim), BF16)],
        axis=0,
    )
    first = 3 * rows
    count = past_count(new_ref.shape[1] - first, heads)
    halves = count // LANES
    block = heads * halves
    gates = []
    for f in range(far):
        parts = new_ref[f, first + 2 * count :, :].astype(F32)
        gates.append(parts[0:block] + parts[block : 2 * block] + parts[2 * block : 3 * block])
    lse_lanes = jnp.zeros(shape, F32)
    for h in range(heads):
        query = shared_ref[:, :, h * head_dim : (h + 1) * head_dim].reshape(near * rows, head_dim)
        scores = []
        for f in range(far):
            row = jnp.concatenate(
                [gates[f][half * heads + h : half * heads + h + 1, :] for half in range(halves)],
                axis=1,
            )
            scores.append(dot_t(query, new_ref[f, first : first + count, :]) * scale + row)
        fresh = dot_t(query, new_keys) * scale - key_run[h : h + 1, :]
        fresh = jnp.where(visible, fresh, -jnp.inf)
        top = jnp.maximum(
            jnp.max(functools.reduce(jnp.maximum, scores), axis=-1, keepdims=True),
            jnp.max(fresh, axis=-1, keepdims=True),
        )
        fresh = jnp.exp(fresh - top)
        summed = jnp.dot(fresh.astype(BF16), new_values, preferred_element_type=F32)
        wide = jnp.zeros(scores[0].shape, F32)
        for f in range(far):
            exponent = jnp.exp(scores[f] - top)
            wide = wide + exponent
            summed = summed + jnp.dot(
                exponent.astype(BF16),
                new_ref[f, first + count : first + 2 * count, :],
                preferred_element_type=F32,
            )
        total = jnp.sum(wide, axis=-1, keepdims=True) + jnp.sum(fresh, axis=-1, keepdims=True)
        result = (summed * (1.0 / total)).astype(BF16)
        out_ref[:, :, h * head_dim : (h + 1) * head_dim] = result.reshape(near, rows, head_dim)
        lse_lanes = jnp.where(lane == h, top + jnp.log(total), lse_lanes)
    lse_lanes = lse_lanes + jnp.where(lane < heads, row_run, 0.0)
    out_ref[:, :, width:] = (
        pack_lanes(lse_lanes, heads).astype(BF16).reshape(near, rows, LANES)
    )


def attend(place, shared, new_blocks, heads, sizes):
    vmem = pl.BlockSpec(memory_space=pltpu.VMEM)
    return pl.pallas_call(
        functools.partial(attend_kernel, heads, sizes),
        out_shape=jax.ShapeDtypeStruct(shared.shape, BF16),
        in_specs=[pl.BlockSpec(memory_space=pltpu.SMEM), vmem, vmem],
        out_specs=vmem,
        compiler_params=room(),
        cost_estimate=cost(4.0, 1 << 20),
        name="attend",
    )(place, shared, new_blocks)


def merge_kernel(heads, back_ref, wo_ref, out_ref):
    near, rows = back_ref.shape[0], back_ref.shape[1]
    width = back_ref.shape[2] - LANES
    head_dim = width // heads
    lse = unpack_lanes(back_ref[:, :, width:].reshape(near * rows, LANES).astype(F32), heads)
    blocks = [lse[i * rows : (i + 1) * rows, :] for i in range(near)]
    top = functools.reduce(jnp.maximum, blocks)
    weights = [jnp.exp(b - top) for b in blocks]
    inverse = 1.0 / functools.reduce(jnp.add, weights)
    weights = [w * inverse for w in weights]
    merged = []
    for h in range(heads):
        summed = jnp.zeros((rows, head_dim), F32)
        for i in range(near):
            part = back_ref[i, :, h * head_dim : (h + 1) * head_dim].astype(F32)
            summed = summed + part * weights[i][:, h : h + 1]
        merged.append(summed.astype(BF16))
    attention = jnp.concatenate(merged, axis=1)
    out_ref[...] = jnp.dot(attention, wo_ref[...], preferred_element_type=F32).astype(BF16)


def merge(back, out_weight, heads):
    _, rows, _ = back.shape
    vmem = pl.BlockSpec(memory_space=pltpu.VMEM)
    return pl.pallas_call(
        functools.partial(merge_kernel, heads),
        out_shape=jax.ShapeDtypeStruct((rows, out_weight.shape[1]), BF16),
        in_specs=[vmem, vmem],
        out_specs=vmem,
        compiler_params=room(),
        cost_estimate=cost(2.0, 2 << 20),
        name="merge",
    )(back, out_weight)


def final_kernel(one_ref, two_ref, gain_ref, out_ref):
    mixed = one_ref[...].astype(F32) + two_ref[...].astype(F32)
    out_ref[...] = rms_scale(mixed, gain_ref[...]).astype(BF16)


def final(one, two, gain):
    vmem = pl.BlockSpec(memory_space=pltpu.VMEM)
    return pl.pallas_call(
        final_kernel,
        out_shape=jax.ShapeDtypeStruct(one.shape, BF16),
        in_specs=[vmem] * 3,
        out_specs=vmem,
        compiler_params=room(),
        cost_estimate=cost(0.5, 1 << 17),
        name="final",
    )(one, two, gain.reshape(1, -1))


def dec_kernel(
    lengths_ref,
    tok_hbm,
    gain_ref,
    wq_hbm,
    wk_hbm,
    wv_hbm,
    wg_ref,
    bias_ref,
    keys_hbm,
    values_hbm,
    gate_hbm,
    wo_hbm,
    out_ref,
    wo_ref,
    tok_ref,
    wq_ref,
    wk_ref,
    wv_ref,
    keys_ref,
    values_ref,
    gate_ref,
    rows_ref,
    query_ref,
    run_ref,
    bias_rows_ref,
    score_ref,
    result_ref,
    sems,
):
    seqs, new, _ = tok_ref.shape
    width = wq_ref.shape[1]
    past, head_dim = keys_ref.shape[1], keys_ref.shape[2]
    heads = width // head_dim
    scale = head_dim ** (-0.5)
    each = heads * new
    total_rows = seqs * each
    moves = (
        (tok_hbm, tok_ref),
        (wq_hbm, wq_ref),
        (wk_hbm, wk_ref),
        (wv_hbm, wv_ref),
        (gate_hbm, gate_ref),
        (keys_hbm, keys_ref),
        (values_hbm, values_ref),
        (wo_hbm, wo_ref),
    )
    copies = [pltpu.make_async_copy(src, dst, sems.at[n]) for n, (src, dst) in enumerate(moves)]
    for copy in copies:
        copy.start()
    copies[0].wait()
    for s in range(seqs):
        rows_ref[s * new : (s + 1) * new, :] = tok_ref[s].astype(F32)
    normed = rms_scale(rows_ref[...], gain_ref[...]).astype(BF16)
    rows = seqs * new
    logits = dot_t(normed, wg_ref[...]) + bias_ref[...]
    gates = jnp.minimum(logits, 0.0) - jnp.log1p(jnp.exp(-jnp.abs(logits)))
    lane = lane_index((rows, LANES))
    row = row_index((rows, LANES))
    run = jnp.zeros((rows, LANES), F32)
    for h in range(heads):
        run = jnp.where(lane == h, gates[:, h : h + 1], run)
    step = 1
    while step < new:
        run = run + jnp.where(row % new >= step, pltpu.roll(run, step, 0), 0.0)
        step *= 2
    copies[1].wait()
    queries = jnp.dot(normed, wq_ref[...], preferred_element_type=F32)
    copies[2].wait()
    pad = jnp.zeros((LANES - rows, head_dim), BF16)
    new_keys = jnp.dot(normed, wk_ref[...], preferred_element_type=F32).astype(BF16)
    copies[3].wait()
    new_values = jnp.dot(normed, wv_ref[...], preferred_element_type=F32).astype(BF16)
    new_keys = jnp.concatenate([new_keys, pad], axis=0)
    new_values = jnp.concatenate([new_values, pad], axis=0)
    copies[4].wait()
    for s in range(seqs):
        for h in range(heads):
            at = s * each + h * new
            query_ref[at : at + new, :] = queries[
                s * new : (s + 1) * new, h * head_dim : (h + 1) * head_dim
            ]
            run_ref[at : at + new, :] = run[s * new : (s + 1) * new, :]
            bias_rows_ref[at : at + new, :] = jnp.broadcast_to(
                gate_ref[s, h : h + 1, :], (new, past)
            )
    query = query_ref[...].astype(BF16)
    copies[5].wait()
    for s in range(seqs):
        score_ref[s * each : (s + 1) * each, :] = dot_t(
            query[s * each : (s + 1) * each, :], keys_ref[s]
        )
    lane = lane_index((total_rows, LANES))
    row = row_index((total_rows, LANES))
    head = (row // new) % heads
    row_run = jnp.sum(jnp.where(lane == head, run_ref[...], 0.0), axis=-1, keepdims=True)
    length = jnp.zeros((total_rows, LANES), jnp.int32)
    for s in range(seqs):
        length = jnp.where(row // each == s, lengths_ref[s], length)
    length = length[:, 0:1]
    slot = lane_index((total_rows, past))
    gate = bias_rows_ref[...]
    last = jnp.sum(jnp.where(slot == length - 1, gate, 0.0), axis=-1, keepdims=True)
    scores = score_ref[...] * scale + (last - gate) + row_run
    scores = jnp.where(slot < length, scores, -jnp.inf)
    by_key = jnp.transpose(
        jnp.concatenate([run, jnp.zeros((LANES - rows, LANES), F32)], axis=0)
    )
    key_run = jnp.zeros((total_rows, LANES), F32)
    for h in range(heads):
        key_run = jnp.where(head == h, by_key[h : h + 1, :], key_run)
    fresh = dot_t(query, new_keys) * scale + row_run - key_run
    visible = (lane // new == row // each) & (lane % new <= row % new)
    fresh = jnp.where(visible, fresh, -jnp.inf)
    top = jnp.maximum(
        jnp.max(scores, axis=-1, keepdims=True), jnp.max(fresh, axis=-1, keepdims=True)
    )
    weights = jnp.exp(scores - top)
    fresh = jnp.exp(fresh - top)
    total = jnp.sum(weights, axis=-1, keepdims=True) + jnp.sum(fresh, axis=-1, keepdims=True)
    inverse = 1.0 / total
    weights = weights.astype(BF16)
    summed = jnp.dot(fresh.astype(BF16), new_values, preferred_element_type=F32)
    copies[6].wait()
    for s in range(seqs):
        part = slice(s * each, (s + 1) * each)
        attention = summed[part, :] + jnp.dot(
            weights[part, :], values_ref[s], preferred_element_type=F32
        )
        attention = attention * inverse[part, :]
        for h in range(heads):
            result_ref[s * new : (s + 1) * new, h * head_dim : (h + 1) * head_dim] = attention[
                h * new : (h + 1) * new, :
            ]
    copies[7].wait()
    out_ref[...] = jnp.dot(
        result_ref[...].astype(BF16), wo_ref[...], preferred_element_type=F32
    ).astype(BF16)


def decode(tokens, gain, wq, wk, wv, wg, bias, keys, values, gate, lengths, wo):
    seqs, new, model = tokens.shape
    heads = bias.shape[0]
    width, head_dim = wq.shape[1], wk.shape[1]
    past = keys.shape[1]
    each = heads * new
    hbm = pl.BlockSpec(memory_space=pl.ANY)
    vmem = pl.BlockSpec(memory_space=pltpu.VMEM)
    return pl.pallas_call(
        dec_kernel,
        out_shape=jax.ShapeDtypeStruct((seqs * new, wo.shape[1]), BF16),
        in_specs=[
            pl.BlockSpec(memory_space=pltpu.SMEM),
            hbm,
            vmem,
            hbm,
            hbm,
            hbm,
            vmem,
            vmem,
            hbm,
            hbm,
            hbm,
            hbm,
        ],
        out_specs=vmem,
        scratch_shapes=[
            pltpu.VMEM(wo.shape, BF16),
            pltpu.VMEM((seqs, new, model), BF16),
            pltpu.VMEM((model, width), BF16),
            pltpu.VMEM((model, head_dim), BF16),
            pltpu.VMEM((model, head_dim), BF16),
            pltpu.VMEM((seqs, past, head_dim), BF16),
            pltpu.VMEM((seqs, past, head_dim), BF16),
            pltpu.VMEM((seqs, heads, past), F32),
            pltpu.VMEM((seqs * new, model), F32),
            pltpu.VMEM((seqs * each, head_dim), F32),
            pltpu.VMEM((seqs * each, LANES), F32),
            pltpu.VMEM((seqs * each, past), F32),
            pltpu.VMEM((seqs * each, past), F32),
            pltpu.VMEM((seqs * new, width), F32),
            pltpu.SemaphoreType.DMA((8,)),
        ],
        cost_estimate=cost(6.0, 8 << 20),
        name="decode",
    )(
        lengths,
        tokens,
        gain.reshape(1, model),
        wq,
        wk,
        wv,
        wg.T,
        bias.reshape(1, heads),
        keys.reshape(seqs, past, head_dim),
        values.reshape(seqs, past, head_dim),
        gate,
        wo,
    )


def groups(sizes, cores):
    far = FAR
    deep, across = sizes[0] // far, sizes[1] // far
    alike, block = {}, {}
    for z in range(sizes[0]):
        for y in range(sizes[1]):
            for core in range(cores):
                index = (z * sizes[1] + y) * cores + core
                first = core % 2 == 0
                alike.setdefault((core, z // deep if first else y // across), []).append(index)
                block.setdefault(
                    (core, z % deep if first else y % across, y if first else z), []
                ).append(index)
    return far, list(alike.values()), list(block.values())


def exchange(x, members):
    return lax.all_to_all(
        x, PART, split_axis=0, concat_axis=0, axis_index_groups=members, tiled=True
    )


def swapped(x):
    return lax.ppermute(x, "tp", [(0, 1), (1, 0)])


def layer(
    piece_tokens,
    dec_tokens,
    norm_gain,
    query_weight,
    key_weight,
    value_weight,
    gate_weight,
    gate_bias,
    out_weight,
    out_gain,
    past_keys,
    past_values,
    past_gate,
    dec_keys,
    dec_values,
    dec_gate,
    dec_lengths,
):
    heads = gate_bias.shape[0]
    sizes = (lax.axis_size("z"), lax.axis_size("y"))
    far, alike, block = groups(sizes, lax.axis_size("tp"))
    near = sizes[0] * sizes[1] // far
    z, y, core = (lax.axis_index(name) for name in PART)
    deep, across = sizes[0] // far, sizes[1] // far
    place = jnp.stack(
        [
            jnp.where(core == 0, z // deep, y // across),
            jnp.where(core == 0, (z % deep) * sizes[1] + y, z * across + y % across),
            core,
        ]
    ).astype(jnp.int32)
    count, _, head_dim = past_keys.shape

    shares, new_rows = piece_projections(
        piece_tokens, norm_gain, query_weight, key_weight, value_weight, gate_weight, gate_bias, near
    )
    shared = exchange(shares, alike)
    past_gate, shared = lax.optimization_barrier((past_gate, shared))
    past = packed_past(
        past_keys.reshape(count, head_dim), past_values.reshape(count, head_dim), past_gate
    )
    payload = run_payload(shared, new_rows, past, far)
    new_blocks = exchange(payload, block)
    partials = attend(place, shared, new_blocks, heads, sizes)
    back = exchange(partials, alike)
    dec_partial = decode(
        dec_tokens,
        norm_gain,
        query_weight,
        key_weight,
        value_weight,
        gate_weight,
        gate_bias,
        dec_keys,
        dec_values,
        dec_gate,
        dec_lengths,
        out_weight,
    )
    dec_rows = final(dec_partial, swapped(dec_partial), out_gain)
    piece_partial = merge(back, out_weight, heads)
    piece_rows = final(piece_partial, swapped(piece_partial), out_gain)
    return piece_rows, dec_rows.reshape(dec_tokens.shape)


def solution(mesh):
    finer = Mesh(
        mesh.devices.reshape(mesh.shape["dp"], 8, 8, mesh.shape["tp"]),
        ("dp", "z", "y", "tp"),
    )
    in_specs = (
        P(DP_KV, None),
        P(DP_KV, None, None),
        P(),
        P(None, "tp"),
        P(None, "tp"),
        P(None, "tp"),
        P(None, "tp"),
        P("tp"),
        P("tp", None),
        P(),
        P(DP_KV, "tp", None),
        P(DP_KV, "tp", None),
        P("tp", DP_KV),
        P(DP_KV, None, "tp", None),
        P(DP_KV, None, "tp", None),
        P(DP_KV, "tp", None),
        P(DP_KV),
    )
    out_specs = (P(DP_KV, None), P(DP_KV, None, None))
    return jax.shard_map(layer, mesh=finer, in_specs=in_specs, out_specs=out_specs, check_vma=False)
```

profile of v0, /device:TPU:1, one launch (start us, length us, event | category | flops | bytes accessed | tf_op | source)
XLA Modules:
  0.0 77.4 jit_solution(3037715352291981392)
XLA Ops:
  0.6 0.0 copy-start.6
  0.6 0.0 copy-start.2
  0.7 0.0 copy-start.3
  0.7 3.6 %piece_proj.1 = (bf16[16,16,640]{2,1,0:T(8,128)(2,1)}, bf16[48,128]{1,0:T(8,128)(2,1)}) custom-call(bf16[16,2048]{1,0:T(8,128)(2,1)} %tok_hbm.2, f32[1,2048]{1,0:T(1,128)} %bitcast.19, bf16[2048,512]{1,0:T(8,128)(2,1)} %wq_hbm.3, bf16[2048,128]{1,0:T(8,128)(2,1)} %wk_hbm.3, bf16[2048,128]{1,0:T(8,128)(2,1)} %wv_hbm.3, bf16[4,2048]{1,0:T(4,128)(2,1)} %bitcast.17, ...), custom_call_target="tpu_custom_call" | custom-call | flops 45000000 | bytes 3145728 | tf_op jit(solution)/shard_map/piece_proj/pallas_call | solution.py:131
  4.2 28.4 %all_to_all.15.shared_ref = bf16[16,16,640]{2,1,0:T(8,128)(2,1)S(1)} all-to-all(bf16[16,16,640]{2,1,0:T(8,128)(2,1)} %get-tuple-element.6), channel_id=1, replica_groups={{0,2,4,6,8,10,12,14,16,18,20,22,24,26,28,30},{1,3,17,19,33,35,49,51,65,..., dimensions={0} | all-to-all | bytes 655360 | tf_op jit(solution)/shard_map/all_to_all | solution.py:629
  32.6 0.0 copy-done.6
  32.6 0.0 copy-done.2
  32.6 0.0 copy-done.3
  32.6 0.2 pack_past.1.past_ref
  32.9 0.0 copy-start.5
  32.9 0.7 copy-done.5
  33.6 0.9 %run_payload.1 = bf16[4,592,128]{2,1,0:T(8,128)(2,1)} custom-call(bf16[16,16,640]{2,1,0:T(8,128)(2,1)S(1)} %all_to_all.15.shared_ref, bf16[48,128]{1,0:T(8,128)(2,1)S(1)} %copy-done.5, bf16[544,128]{1,0:T(8,128)(2,1)S(1)} %pack_past.1.past_ref), custom_call_target="tpu_custom_call" | custom-call | flops 15000000 | bytes 262144 | tf_op jit(solution)/shard_map/run_payload/pallas_call | solution.py:223
  34.5 8.4 %all-to-all-start.1 = ((bf16[4,592,128]{2,1,0:T(8,128)(2,1)}), bf16[4,592,128]{2,1,0:T(8,128)(2,1)S(1)}, u32[]{:S(2)}, u32[]{:S(2)}) async-start(bf16[4,592,128]{2,1,0:T(8,128)(2,1)} %run_payload.1), calls=%async_computation.1 | async-start | bytes 1212416 | tf_op jit(solution)/shard_map/all_to_all | solution.py:629
  42.9 0.1 pad_add_fusion.place_ref
  43.0 11.1 %all-to-all-done.1.new_ref = bf16[4,592,128]{2,1,0:T(8,128)(2,1)S(1)} async-done(((bf16[4,592,128]{2,1,0:T(8,128)(2,1)}), bf16[4,592,128]{2,1,0:T(8,128)(2,1)S(1)}, u32[]{:S(2)}, u32[]{:S(2)}) %all-to-all-start.1) | async-done | bytes 606240 | tf_op jit(solution)/shard_map/all_to_all | solution.py:629
  54.1 3.9 %attend.1 = bf16[16,16,640]{2,1,0:T(8,128)(2,1)} custom-call(s32[3]{0:T(128)S(1)} %pad_add_fusion.place_ref, bf16[16,16,640]{2,1,0:T(8,128)(2,1)S(1)} %all_to_all.15.shared_ref, bf16[4,592,128]{2,1,0:T(8,128)(2,1)S(1)} %all-to-all-done.1.new_ref), custom_call_target="tpu_custom_call" | custom-call | flops 60000000 | bytes 1048576 | tf_op jit(solution)/shard_map/attend/pallas_call | solution.py:347
  58.0 3.6 %all-to-all-start.2 = ((bf16[16,16,640]{2,1,0:T(8,128)(2,1)}), bf16[16,16,640]{2,1,0:T(8,128)(2,1)S(1)}, u32[]{:S(2)}, u32[]{:S(2)}) async-start(bf16[16,16,640]{2,1,0:T(8,128)(2,1)} %attend.1), calls=%async_computation.2 | async-start | bytes 655360 | tf_op jit(solution)/shard_map/all_to_all | solution.py:629
  61.5 0.0 copy-start
  61.6 6.0 %decode.1.one_ref = bf16[48,2048]{1,0:T(8,128)(2,1)} custom-call(s32[12]{0:T(128)} %lengths_ref.1, bf16[12,4,2048]{2,1,0:T(4,128)(2,1)} %tok_hbm.3, f32[1,2048]{1,0:T(1,128)} %bitcast.20, bf16[2048,512]{1,0:T(8,128)(2,1)} %wq_hbm.3, bf16[2048,128]{1,0:T(8,128)(2,1)} %wk_hbm.3, bf16[2048,128]{1,0:T(8,128)(2,1)} %wv_hbm.3, bf16[4,2048]{1,0:T(4,128)(2,1)} %bitcast.18, ...), custom_call_target="tpu_custom_call" | custom-call | flops 90000000 | bytes 8388608 | tf_op jit(solution)/shard_map/decode/pallas_call | solution.py:559
  67.5 0.0 copy-start.1
  67.5 0.0 copy-start.4
  67.6 3.2 %collective-permute-start.1 = (bf16[48,2048]{1,0:T(8,128)(2,1)}, bf16[48,2048]{1,0:T(8,128)(2,1)S(1)}, u32[]{:S(2)}, u32[]{:S(2)}) collective-permute-start(bf16[48,2048]{1,0:T(8,128)(2,1)} %decode.1.one_ref), channel_id=1, source_target_pairs={{0,1},{1,0},{2,3},{3,2},{4,5},{5,4},{6,7},{7,6},{8,9},{9,8},{10,11... | collective-permute-start | bytes 589832 | tf_op jit(solution)/shard_map/ppermute | solution.py:635
  70.8 1.9 %all-to-all-done.2.back_ref = bf16[16,16,640]{2,1,0:T(8,128)(2,1)S(1)} async-done(((bf16[16,16,640]{2,1,0:T(8,128)(2,1)}), bf16[16,16,640]{2,1,0:T(8,128)(2,1)S(1)}, u32[]{:S(2)}, u32[]{:S(2)}) %all-to-all-start.2) | async-done | bytes 327712 | tf_op jit(solution)/shard_map/all_to_all | solution.py:629
  72.7 0.7 merge.1.one_ref
  73.5 1.9 %collective-permute-start = (bf16[16,2048]{1,0:T(8,128)(2,1)S(1)}, bf16[16,2048]{1,0:T(8,128)(2,1)S(1)}, u32[]{:S(2)}, u32[]{:S(2)}) collective-permute-start(bf16[16,2048]{1,0:T(8,128)(2,1)S(1)} %merge.1.one_ref), channel_id=1, source_target_pairs={{0,1},{1,0},{2,3},{3,2},{4,5},{5,4},{6,7},{7,6},{8,9},{9,8},{10,11... | collective-permute-start | bytes 196616 | tf_op jit(solution)/shard_map/ppermute | solution.py:635
  75.4 0.0 collective-permute-done.1.two_ref
  75.4 0.0 copy-done.1
  75.4 0.0 copy-done.4
  75.4 0.2 final.3
  75.6 0.8 reshape.38
  76.3 0.3 collective-permute-done.two_ref
  76.6 0.7 final.2
  (1 shorter events, 0.0 us)
Async XLA Ops:
  0.6 32.0 %copy-start.6 = (f32[4,256]{1,0:T(4,128)S(1)}, f32[4,256]{1,0:T(4,128)}, u32[]{:S(2)}) copy-start(f32[4,256]{1,0:T(4,128)} %gate_ref) | copy-start | bytes 12292
  0.6 32.0 %copy-start.2 = (bf16[256,1,128]{2,0,1:T(8,128)(2,1)S(1)}, bf16[256,1,128]{2,0,1:T(8,128)(2,1)}, u32[]{:S(2)}) copy-start(bf16[256,1,128]{2,0,1:T(8,128)(2,1)} %param.27) | copy-start | bytes 196612
  0.7 32.0 %copy-start.3 = (bf16[256,1,128]{2,0,1:T(8,128)(2,1)S(1)}, bf16[256,1,128]{2,0,1:T(8,128)(2,1)}, u32[]{:S(2)}) copy-start(bf16[256,1,128]{2,0,1:T(8,128)(2,1)} %param.28) | copy-start | bytes 196612
  32.9 0.7 copy-start.5
  34.5 19.6 %all-to-all-start.1 = ((bf16[4,592,128]{2,1,0:T(8,128)(2,1)}), bf16[4,592,128]{2,1,0:T(8,128)(2,1)S(1)}, u32[]{:S(2)}, u32[]{:S(2)}) async-start(bf16[4,592,128]{2,1,0:T(8,128)(2,1)} %run_payload.1), calls=%async_computation.1 | async-start | bytes 1212416 | tf_op jit(solution)/shard_map/all_to_all | solution.py:629
  58.0 14.8 %all-to-all-start.2 = ((bf16[16,16,640]{2,1,0:T(8,128)(2,1)}), bf16[16,16,640]{2,1,0:T(8,128)(2,1)S(1)}, u32[]{:S(2)}, u32[]{:S(2)}) async-start(bf16[16,16,640]{2,1,0:T(8,128)(2,1)} %attend.1), calls=%async_computation.2 | async-start | bytes 655360 | tf_op jit(solution)/shard_map/all_to_all | solution.py:629
  61.5 11.2 %copy-start = (bf16[512,2048]{1,0:T(8,128)(2,1)S(1)}, bf16[512,2048]{1,0:T(8,128)(2,1)}, u32[]{:S(2)}) copy-start(bf16[512,2048]{1,0:T(8,128)(2,1)} %wo_hbm.1) | copy-start | bytes 6291460
  67.5 7.9 %copy-start.1 = (bf16[48,2048]{1,0:T(8,128)(2,1)S(1)}, bf16[48,2048]{1,0:T(8,128)(2,1)}, u32[]{:S(2)}) copy-start(bf16[48,2048]{1,0:T(8,128)(2,1)} %decode.1.one_ref) | copy-start | bytes 589828
  67.5 7.9 %copy-start.4 = (f32[2048]{0:T(1024)S(1)}, f32[2048]{0:T(1024)}, u32[]{:S(2)}) copy-start(f32[2048]{0:T(1024)} %param.26) | copy-start | bytes 24580
  67.6 7.8 %collective-permute-start.1 = (bf16[48,2048]{1,0:T(8,128)(2,1)}, bf16[48,2048]{1,0:T(8,128)(2,1)S(1)}, u32[]{:S(2)}, u32[]{:S(2)}) collective-permute-start(bf16[48,2048]{1,0:T(8,128)(2,1)} %decode.1.one_ref), channel_id=1, source_target_pairs={{0,1},{1,0},{2,3},{3,2},{4,5},{5,4},{6,7},{7,6},{8,9},{9,8},{10,11... | collective-permute-start | bytes 589832 | tf_op jit(solution)/shard_map/ppermute | solution.py:635
  73.5 3.1 %collective-permute-start = (bf16[16,2048]{1,0:T(8,128)(2,1)S(1)}, bf16[16,2048]{1,0:T(8,128)(2,1)S(1)}, u32[]{:S(2)}, u32[]{:S(2)}) collective-permute-start(bf16[16,2048]{1,0:T(8,128)(2,1)S(1)} %merge.1.one_ref), channel_id=1, source_target_pairs={{0,1},{1,0},{2,3},{3,2},{4,5},{5,4},{6,7},{7,6},{8,9},{9,8},{10,11... | collective-permute-start | bytes 196616 | tf_op jit(solution)/shard_map/ppermute | solution.py:635
where the time goes:
time: 77.9 us; the launch traced here: 77.4 us
  blocking collectives  28.4 us (36%)
  starting transfers between devices  17.1 us (22%)
  Pallas kernels  16.2 us (21%)
  waiting for transfers between devices  13.3 us (17%)
  local copies, waits for them, and re-layouts  1.49 us (2%)
  between operations  0.78 us (1%)
    all_to_all x1, blocking collectives, exchange(): lax.all_to_all(x, PART, split_axis=0, concat_axis=0, axis_index_groups=me...  28.4 us
    all_to_all x2, waiting for transfers between devices, exchange(): lax.all_to_all(x, PART, split_axis=0, concat_axis=0, axis_index_groups=me...  13 us
    all_to_all x2, starting transfers between devices, exchange(): lax.all_to_all(x, PART, split_axis=0, concat_axis=0, axis_index_groups=me...  12 us
    pallas_call x1, Pallas kernels, decode(): pl.pallas_call(dec_kernel, out_shape=jax.ShapeDtypeStruct((seqs * new, wo...  5.97 us
    ppermute x2, starting transfers between devices, swapped(): return lax.ppermute(x, 'tp', [(0, 1), (1, 0)])  5.14 us
    pallas_call x1, Pallas kernels, attend(): pl.pallas_call(functools.partial(attend_kernel, heads, sizes), out_shape=...  3.89 us
    pallas_call x1, Pallas kernels, piece_projections(): pl.pallas_call(functools.partial(proj_kernel, heads), out_shape=(jax.Shap...  3.57 us
  transfers between devices with their start and end apart: 4, of which 3 were waited for; matrix products, arithmetic and copies ran while one was open for 1% of the time, Pallas kernels for 9%

commit v1 on v0

--- a/solution.py
+++ b/solution.py
@@ -57,32 +57,38 @@
     return x + pltpu.roll(x, LANES - heads, 1) + pltpu.roll(x, LANES - 2 * heads, 1)
 
 
+def my_place(sizes, far):
+    z, y, core = (lax.axis_index(name) for name in PART)
+    deep, across = sizes[0] // far, sizes[1] // far
+    first = core == 0
+    return (
+        jnp.where(first, z // deep, y // across),
+        jnp.where(first, (z % deep) * sizes[1] + y, z * across + y % across),
+        core,
+    )
+
+
+def fold_rows(x):
+    half = x.shape[0] // 2
+    upper, lower = x[0:half, :], x[half:, :]
+    return jnp.where(lane_index(upper.shape) < 16, upper, pltpu.roll(lower, 16, 1))
+
+
+def unfold_rows(x):
+    return x, pltpu.roll(x, LANES - 16, 1)
+
+
 def proj_kernel(
-    heads,
-    tok_hbm,
-    gain_ref,
-    wq_hbm,
-    wk_hbm,
-    wv_hbm,
-    wg_ref,
-    bias_ref,
-    share_ref,
-    new_ref,
-    tok_ref,
-    wq_ref,
-    wk_ref,
-    wv_ref,
-    sems,
+    heads, tok_hbm, gain_ref, wq_hbm, wg_ref, bias_ref, share_ref, tok_ref, wq_ref, sems
 ):
     model, width = wq_ref.shape
-    pieces = sems.shape[0] - 3
+    pieces = sems.shape[0] - 1
     depth = model // pieces
     moves = [(tok_hbm, tok_ref)]
     moves += [
         (wq_hbm.at[pl.ds(n * depth, depth)], wq_ref.at[pl.ds(n * depth, depth)])
         for n in range(pieces)
     ]
-    moves += [(wk_hbm, wk_ref), (wv_hbm, wv_ref)]
     copies = [pltpu.make_async_copy(src, dst, sems.at[n]) for n, (src, dst) in enumerate(moves)]
     for copy in copies:
         copy.start()
@@ -100,7 +106,7 @@
     while step < rows:
         run = run + jnp.where(row >= step, pltpu.roll(run, step, 0), 0.0)
         step *= 2
-    packed = pack_lanes(run, heads).astype(BF16)
+    packed = fold_rows(pack_lanes(run, heads)).astype(BF16)
     queries = jnp.zeros((rows, width), F32)
     for n in range(pieces):
         copies[1 + n].wait()
@@ -110,58 +116,67 @@
             preferred_element_type=F32,
         )
     queries = queries.astype(BF16)
+    head_dim = width // heads
     for slot in range(share_ref.shape[0]):
-        share_ref[slot, :, 0:width] = queries
-        share_ref[slot, :, width:] = packed
-    copies[1 + pieces].wait()
-    new_ref[0:rows, :] = jnp.dot(normed, wk_ref[...], preferred_element_type=F32).astype(BF16)
-    copies[2 + pieces].wait()
-    new_ref[rows : 2 * rows, :] = jnp.dot(
-        normed, wv_ref[...], preferred_element_type=F32
-    ).astype(BF16)
-    new_ref[2 * rows :, :] = packed
-
-
-def piece_projections(tokens, gain, wq, wk, wv, wg, bias, near):
+        for h in range(heads):
+            share_ref[slot, h * rows : (h + 1) * rows, :] = queries[
+                :, h * head_dim : (h + 1) * head_dim
+            ]
+        share_ref[slot, heads * rows :, :] = packed
+
+
+def piece_queries(tokens, gain, wq, wg, bias, near):
     rows, model = tokens.shape
     heads = bias.shape[0]
-    width, head_dim = wq.shape[1], wk.shape[1]
+    width = wq.shape[1]
     hbm = pl.BlockSpec(memory_space=pl.ANY)
     vmem = pl.BlockSpec(memory_space=pltpu.VMEM)
     return pl.pallas_call(
         functools.partial(proj_kernel, heads),
-        out_shape=(
-            jax.ShapeDtypeStruct((near, rows, width + LANES), BF16),
-            jax.ShapeDtypeStruct((3 * rows, head_dim), BF16),
+        out_shape=jax.ShapeDtypeStruct(
+            (near, heads * rows + rows // 2, width // heads), BF16
         ),
-        in_specs=[hbm, vmem, hbm, hbm, hbm, vmem, vmem],
-        out_specs=(vmem, vmem),
+        in_specs=[hbm, vmem, hbm, vmem, vmem],
+        out_specs=vmem,
         scratch_shapes=[
             pltpu.VMEM((rows, model), BF16),
             pltpu.VMEM((model, width), BF16),
-            pltpu.VMEM((model, head_dim), BF16),
-            pltpu.VMEM((model, head_dim), BF16),
-            pltpu.SemaphoreType.DMA((7,)),
+            pltpu.SemaphoreType.DMA((5,)),
         ],
-        cost_estimate=cost(3.0, 3 << 20),
-        name="piece_proj",
-    )(
-        tokens,
-        gain.reshape(1, model),
-        wq,
-        wk,
-        wv,
-        wg.T,
-        bias.reshape(1, heads),
-    )
-
-
-def pack_kernel(heads, pk_hbm, pv_hbm, gate_ref, past_ref, parts_ref, sems):
-    count = pk_hbm.shape[0]
-    moves = [(pk_hbm, past_ref.at[pl.ds(0, count)]), (pv_hbm, past_ref.at[pl.ds(count, count)])]
-    copies = [pltpu.make_async_copy(src, dst, sems.at[n]) for n, (src, dst) in enumerate(moves)]
-    for copy in copies:
-        copy.start()
+        cost_estimate=cost(3.0, 2 << 20),
+        name="piece_queries",
+    )(tokens, gain.reshape(1, model), wq, wg.T, bias.reshape(1, heads))
+
+
+def payload_kernel(
+    heads,
+    sizes,
+    shared_ref,
+    tok_ref,
+    gain_ref,
+    wk_ref,
+    wv_ref,
+    pk_ref,
+    pv_ref,
+    gate_ref,
+    out_ref,
+    parts_ref,
+):
+    rows = tok_ref.shape[0]
+    near = shared_ref.shape[0]
+    tail = heads * rows
+    count = pk_ref.shape[0]
+    normed = rms_scale(tok_ref[...], gain_ref[...]).astype(BF16)
+    keys = jnp.dot(normed, wk_ref[...], preferred_element_type=F32).astype(BF16)
+    values = jnp.dot(normed, wv_ref[...], preferred_element_type=F32).astype(BF16)
+    my_near = my_place(sizes, out_ref.shape[0])[1]
+    mine = shared_ref[my_near, tail:, :].astype(F32)
+    run = jnp.concatenate(unfold_rows(mine), axis=0)
+    totals = jnp.concatenate(
+        [shared_ref[i, tail:, :].astype(F32)[rows // 2 - 1 : rows // 2, :] for i in range(near)],
+        axis=0,
+    )
+    run = jnp.where(lane_index(run.shape) < 16, run, totals).astype(BF16)
     halves = count // LANES
     block = heads * halves
     parts_ref[...] = jnp.zeros_like(parts_ref)
@@ -169,27 +184,45 @@
         for half in range(halves):
             at = n * block + half * heads
             parts_ref[at : at + heads, :] = part[:, half * LANES : (half + 1) * LANES]
-    past_ref[2 * count :, :] = parts_ref[...].astype(BF16)
-    for copy in copies:
-        copy.wait()
-
-
-def packed_past(past_keys, past_values, past_gate):
+    parts = parts_ref[...].astype(BF16)
+    first = 3 * rows
+    for slot in range(out_ref.shape[0]):
+        out_ref[slot, 0:rows, :] = keys
+        out_ref[slot, rows : 2 * rows, :] = values
+        out_ref[slot, 2 * rows : first, :] = run
+        out_ref[slot, first : first + count, :] = pk_ref[...]
+        out_ref[slot, first + count : first + 2 * count, :] = pv_ref[...]
+        out_ref[slot, first + 2 * count :, :] = parts
+
+
+def block_payload(sizes, shared, tokens, gain, wk, wv, past_keys, past_values, past_gate, far):
+    rows, model = tokens.shape
+    assert shared.shape[0] == rows
     count, head_dim = past_keys.shape
     heads = past_gate.shape[0]
     gate_rows = -(-3 * heads * (count // LANES) // 16) * 16
-    hbm = pl.BlockSpec(memory_space=pl.ANY)
     vmem = pl.BlockSpec(memory_space=pltpu.VMEM)
     return pl.pallas_call(
-        functools.partial(pack_kernel, heads),
-        out_shape=jax.ShapeDtypeStruct((2 * count + gate_rows, head_dim), BF16),
-        in_specs=[hbm, hbm, vmem],
+        functools.partial(payload_kernel, heads, sizes),
+        out_shape=jax.ShapeDtypeStruct(
+            (far, 3 * rows + 2 * count + gate_rows, head_dim), BF16
+        ),
+        in_specs=[vmem] * 8,
         out_specs=vmem,
-        scratch_shapes=[pltpu.VMEM((gate_rows, LANES), F32), pltpu.SemaphoreType.DMA((2,))],
+        scratch_shapes=[pltpu.VMEM((gate_rows, LANES), F32)],
         compiler_params=room(),
-        cost_estimate=cost(2.0, 1 << 18),
-        name="pack_past",
-    )(past_keys, past_values, past_gate)
+        cost_estimate=cost(2.0, 2 << 20),
+        name="block_payload",
+    )(
+        shared,
+        tokens,
+        gain.reshape(1, model),
+        wk,
+        wv,
+        past_keys,
+        past_values,
+        past_gate,
+    )
 
 
 def room():
@@ -200,35 +233,6 @@
     return pl.CostEstimate(
         flops=int(micros * 15e6), bytes_accessed=int(moved), transcendentals=0
     )
-
-
-def run_kernel(shared_ref, new_ref, past_ref, out_ref):
-    near, rows = shared_ref.shape[0], shared_ref.shape[1]
-    width = shared_ref.shape[2] - LANES
-    totals = jnp.concatenate(
-        [shared_ref[i, :, width:].astype(F32)[rows - 1 : rows, :] for i in range(near)], axis=0
-    )
-    run = new_ref[2 * rows :, :].astype(F32)
-    run = jnp.where(lane_index(run.shape) < 16, run, pltpu.roll(totals, 16, 1)).astype(BF16)
-    for slot in range(out_ref.shape[0]):
-        out_ref[slot, 0 : 2 * rows, :] = new_ref[0 : 2 * rows, :]
-        out_ref[slot, 2 * rows : 3 * rows, :] = run
-        out_ref[slot, 3 * rows :, :] = past_ref[...]
-
-
-def run_payload(shared, new_rows, past, far):
-    near, rows, _ = shared.shape
-    assert near == rows
-    vmem = pl.BlockSpec(memory_space=pltpu.VMEM)
-    return pl.pallas_call(
-        run_kernel,
-        out_shape=jax.ShapeDtypeStruct((far, 3 * rows + past.shape[0], LANES), BF16),
-        in_specs=[vmem, vmem, vmem],
-        out_specs=vmem,
-        compiler_params=room(),
-        cost_estimate=cost(1.0, 1 << 18),
-        name="run_payload",
-    )(shared, new_rows, past)
 
 
 def dot_t(a, b):
@@ -242,13 +246,13 @@
     return count
 
 
-def attend_kernel(heads, sizes, place_ref, shared_ref, new_ref, out_ref):
-    near, rows = shared_ref.shape[0], shared_ref.shape[1]
+def attend_kernel(heads, sizes, shared_ref, new_ref, out_ref):
+    near, tail = shared_ref.shape[0], shared_ref.shape[1] * (2 * heads) // (2 * heads + 1)
+    rows = tail // heads
     far, head_dim = new_ref.shape[0], new_ref.shape[2]
     scale = head_dim ** (-0.5)
-    width = heads * head_dim
-    my_far, my_near = place_ref[0], place_ref[1]
-    across, core = sizes[1] // far, place_ref[2]
+    my_far, my_near, core = my_place(sizes, far)
+    across = sizes[1] // far
 
     def block_place(block, alike):
         by_z = block * near + alike
@@ -274,13 +278,17 @@
         axis=0,
     )
     key_run = jnp.transpose(key_run)
-    local = unpack_lanes(
-        shared_ref[:, :, width:].reshape(near * rows, LANES).astype(F32), heads
-    )
-    row_run = jnp.concatenate(
-        [local[i * rows : (i + 1) * rows, :] + before[8 + i : 9 + i, :] for i in range(near)],
-        axis=0,
-    )
+    half = rows // 2
+    upper, lower = (
+        unpack_lanes(x, heads)
+        for x in unfold_rows(shared_ref[:, tail:, :].astype(F32).reshape(near * half, LANES))
+    )
+    row_runs = []
+    for i in range(near):
+        start = before[8 + i : 9 + i, :]
+        row_runs.append(upper[i * half : (i + 1) * half, :] + start)
+        row_runs.append(lower[i * half : (i + 1) * half, :] + start)
+    row_run = jnp.concatenate(row_runs, axis=0)
     shape = (near * rows, LANES)
     row = row_index(shape)
     row_place = block_place(my_far, row // rows) * rows + row % rows
@@ -307,7 +315,7 @@
         gates.append(parts[0:block] + parts[block : 2 * block] + parts[2 * block : 3 * block])
     lse_lanes = jnp.zeros(shape, F32)
     for h in range(heads):
-        query = shared_ref[:, :, h * head_dim : (h + 1) * head_dim].reshape(near * rows, head_dim)
+        query = shared_ref[:, h * rows : (h + 1) * rows, :].reshape(near * rows, head_dim)
         scores = []
         for f in range(far):
             row = jnp.concatenate(
@@ -334,33 +342,44 @@
             )
         total = jnp.sum(wide, axis=-1, keepdims=True) + jnp.sum(fresh, axis=-1, keepdims=True)
         result = (summed * (1.0 / total)).astype(BF16)
-        out_ref[:, :, h * head_dim : (h + 1) * head_dim] = result.reshape(near, rows, head_dim)
+        out_ref[:, h * rows : (h + 1) * rows, :] = result.reshape(near, rows, head_dim)
         lse_lanes = jnp.where(lane == h, top + jnp.log(total), lse_lanes)
     lse_lanes = lse_lanes + jnp.where(lane < heads, row_run, 0.0)
-    out_ref[:, :, width:] = (
-        pack_lanes(lse_lanes, heads).astype(BF16).reshape(near, rows, LANES)
-    )
-
-
-def attend(place, shared, new_blocks, heads, sizes):
+    packed = pack_lanes(lse_lanes, heads).reshape(near, 2, half, LANES)
+    folded = jnp.where(
+        lane_index((near * half, LANES)) < 16,
+        packed[:, 0].reshape(near * half, LANES),
+        pltpu.roll(packed[:, 1].reshape(near * half, LANES), 16, 1),
+    )
+    out_ref[:, tail:, :] = folded.astype(BF16).reshape(near, half, LANES)
+
+
+def attend(shared, new_blocks, heads, sizes):
     vmem = pl.BlockSpec(memory_space=pltpu.VMEM)
     return pl.pallas_call(
         functools.partial(attend_kernel, heads, sizes),
         out_shape=jax.ShapeDtypeStruct(shared.shape, BF16),
-        in_specs=[pl.BlockSpec(memory_space=pltpu.SMEM), vmem, vmem],
+        in_specs=[vmem, vmem],
         out_specs=vmem,
         compiler_params=room(),
         cost_estimate=cost(4.0, 1 << 20),
         name="attend",
-    )(place, shared, new_blocks)
-
-
-def merge_kernel(heads, back_ref, wo_ref, out_ref):
-    near, rows = back_ref.shape[0], back_ref.shape[1]
-    width = back_ref.shape[2] - LANES
-    head_dim = width // heads
-    lse = unpack_lanes(back_ref[:, :, width:].reshape(near * rows, LANES).astype(F32), heads)
-    blocks = [lse[i * rows : (i + 1) * rows, :] for i in range(near)]
+    )(shared, new_blocks)
+
+
+def merge_kernel(heads, back_ref, wo_ref, dec_ref, out_ref):
+    near, tail = back_ref.shape[0], back_ref.shape[1] * (2 * heads) // (2 * heads + 1)
+    rows = tail // heads
+    half = rows // 2
+    head_dim = back_ref.shape[2]
+    upper, lower = (
+        unpack_lanes(x, heads)
+        for x in unfold_rows(back_ref[:, tail:, :].astype(F32).reshape(near * half, LANES))
+    )
+    blocks = [
+        jnp.concatenate([x[i * half : (i + 1) * half, :] for x in (upper, lower)], axis=0)
+        for i in range(near)
+    ]
     top = functools.reduce(jnp.maximum, blocks)
     weights = [jnp.exp(b - top) for b in blocks]
     inverse = 1.0 / functools.reduce(jnp.add, weights)
@@ -369,39 +388,52 @@
     for h in range(heads):
         summed = jnp.zeros((rows, head_dim), F32)
         for i in range(near):
-            part = back_ref[i, :, h * head_dim : (h + 1) * head_dim].astype(F32)
+            part = back_ref[i, h * rows : (h + 1) * rows, :].astype(F32)
             summed = summed + part * weights[i][:, h : h + 1]
         merged.append(summed.astype(BF16))
     attention = jnp.concatenate(merged, axis=1)
-    out_ref[...] = jnp.dot(attention, wo_ref[...], preferred_element_type=F32).astype(BF16)
-
-
-def merge(back, out_weight, heads):
-    _, rows, _ = back.shape
+    out_ref[0:rows, :] = jnp.dot(
+        attention, wo_ref[...], preferred_element_type=F32
+    ).astype(BF16)
+    out_ref[rows:, :] = dec_ref[rows:, :]
+
+
+def merge(back, out_weight, dec_partial, heads):
     vmem = pl.BlockSpec(memory_space=pltpu.VMEM)
     return pl.pallas_call(
         functools.partial(merge_kernel, heads),
-        out_shape=jax.ShapeDtypeStruct((rows, out_weight.shape[1]), BF16),
-        in_specs=[vmem, vmem],
+        out_shape=jax.ShapeDtypeStruct(
+            (dec_partial.shape[0], out_weight.shape[1]), BF16
+        ),
+        in_specs=[vmem, vmem, vmem],
         out_specs=vmem,
         compiler_params=room(),
         cost_estimate=cost(2.0, 2 << 20),
         name="merge",
-    )(back, out_weight)
-
-
-def final_kernel(one_ref, two_ref, gain_ref, out_ref):
+    )(back, out_weight, dec_partial)
+
+
+def final_kernel(one_ref, two_ref, gain_ref, piece_ref, dec_ref, held_ref):
     mixed = one_ref[...].astype(F32) + two_ref[...].astype(F32)
-    out_ref[...] = rms_scale(mixed, gain_ref[...]).astype(BF16)
-
-
-def final(one, two, gain):
+    rows = rms_scale(mixed, gain_ref[...])
+    count, new = piece_ref.shape[0], dec_ref.shape[1]
+    piece_ref[...] = rows[0:count, :].astype(BF16)
+    held_ref[...] = rows[count:, :]
+    for s in range(dec_ref.shape[0]):
+        dec_ref[s] = held_ref[s * new : (s + 1) * new, :].astype(BF16)
+
+
+def final(one, two, gain, piece_shape, dec_shape):
     vmem = pl.BlockSpec(memory_space=pltpu.VMEM)
     return pl.pallas_call(
         final_kernel,
-        out_shape=jax.ShapeDtypeStruct(one.shape, BF16),
+        out_shape=(
+            jax.ShapeDtypeStruct(piece_shape, BF16),
+            jax.ShapeDtypeStruct(dec_shape, BF16),
+        ),
         in_specs=[vmem] * 3,
-        out_specs=vmem,
+        out_specs=(vmem, vmem),
+        scratch_shapes=[pltpu.VMEM((one.shape[0] - piece_shape[0], one.shape[1]), F32)],
         compiler_params=room(),
         cost_estimate=cost(0.5, 1 << 17),
         name="final",
@@ -658,28 +690,24 @@
     sizes = (lax.axis_size("z"), lax.axis_size("y"))
     far, alike, block = groups(sizes, lax.axis_size("tp"))
     near = sizes[0] * sizes[1] // far
-    z, y, core = (lax.axis_index(name) for name in PART)
-    deep, across = sizes[0] // far, sizes[1] // far
-    place = jnp.stack(
-        [
-            jnp.where(core == 0, z // deep, y // across),
-            jnp.where(core == 0, (z % deep) * sizes[1] + y, z * across + y % across),
-            core,
-        ]
-    ).astype(jnp.int32)
     count, _, head_dim = past_keys.shape
 
-    shares, new_rows = piece_projections(
-        piece_tokens, norm_gain, query_weight, key_weight, value_weight, gate_weight, gate_bias, near
-    )
+    shares = piece_queries(piece_tokens, norm_gain, query_weight, gate_weight, gate_bias, near)
     shared = exchange(shares, alike)
-    past_gate, shared = lax.optimization_barrier((past_gate, shared))
-    past = packed_past(
-        past_keys.reshape(count, head_dim), past_values.reshape(count, head_dim), past_gate
-    )
-    payload = run_payload(shared, new_rows, past, far)
+    payload = block_payload(
+        sizes,
+        shared,
+        piece_tokens,
+        norm_gain,
+        key_weight,
+        value_weight,
+        past_keys.reshape(count, head_dim),
+        past_values.reshape(count, head_dim),
+        past_gate,
+        far,
+    )
     new_blocks = exchange(payload, block)
-    partials = attend(place, shared, new_blocks, heads, sizes)
+    partials = attend(shared, new_blocks, heads, sizes)
     back = exchange(partials, alike)
     dec_partial = decode(
         dec_tokens,
@@ -695,10 +723,10 @@
         dec_lengths,
         out_weight,
     )
-    dec_rows = final(dec_partial, swapped(dec_partial), out_gain)
-    piece_partial = merge(back, out_weight, heads)
-    piece_rows = final(piece_partial, swapped(piece_partial), out_gain)
-    return piece_rows, dec_rows.reshape(dec_tokens.shape)
+    dec_partial = jnp.pad(dec_partial, ((piece_tokens.shape[0], 0), (0, 0)))
+    partial = merge(back, out_weight, dec_partial, heads)
+    other = swapped(partial)
+    return final(partial, other, out_gain, piece_tokens.shape, dec_tokens.shape)
 
 
 def solution(mesh):

time: 77.9 us -> 76.1 us (0.977)
  blocking collectives: 28.4 us -> 47.7 us
  starting transfers between devices: 17.1 us -> 6.49 us
  waiting for transfers between devices: 13.3 us -> 4.97 us
  Pallas kernels: 16.2 us -> 14.8 us
    all_to_all x1 -> x2, blocking collectives: 28.4 us -> 47.7 us  [exchange(): lax.all_to_all(x, PART, split_axis=0, concat_axis=0, axis_index_groups=me...]
    all_to_all x2 -> x1, waiting for transfers between devices: 13 us -> 3.83 us  [exchange(): lax.all_to_all(x, PART, split_axis=0, concat_axis=0, axis_index_groups=me...]
    all_to_all x2 -> x1, starting transfers between devices: 12 us -> 3.54 us  [exchange(): lax.all_to_all(x, PART, split_axis=0, concat_axis=0, axis_index_groups=me...]
    ppermute x2 -> x1, starting transfers between devices: 5.14 us -> 2.95 us  [swapped(): return lax.ppermute(x, 'tp', [(0, 1), (1, 0)])]
    pallas_call x5 -> x3, Pallas kernels: 5.6 us -> 4.59 us  [the longest x1 3.35 us: piece_queries(): pl.pallas_call(functools.partial(proj_kernel, heads), out_shape=jax.Shape...]
    pad x0 -> x1, local copies, waits for them, and re-layouts: none -> 0.95 us  [layer(): dec_partial = jnp.pad(dec_partial, ((piece_tokens.shape[0], 0), (0, 0)))]
    ppermute x2 -> x1, waiting for transfers between devices: 0.26 us -> 1.14 us  [swapped(): return lax.ppermute(x, 'tp', [(0, 1), (1, 0)])]
  transfers between devices with their start and end apart: 4 -> 2, of which waited for: 3 -> 2; matrix products, arithmetic and copies ran while one was open for 1% -> 1% of each run, Pallas kernels for 9% -> 8%
where the time goes in v1:
time: 76.1 us; the launch traced here: 75.7 us
  blocking collectives  47.7 us (63%)
  Pallas kernels  14.8 us (19%)
  starting transfers between devices  6.49 us (9%)
  waiting for transfers between devices  4.97 us (7%)
  local copies, waits for them, and re-layouts  1 us (1%)
  between operations  0.78 us (1%)
    all_to_all x2, blocking collectives, exchange(): lax.all_to_all(x, PART, split_axis=0, concat_axis=0, axis_index_groups=me...  47.7 us
    pallas_call x1, Pallas kernels, decode(): pl.pallas_call(dec_kernel, out_shape=jax.ShapeDtypeStruct((seqs * new, wo...  5.97 us
    all_to_all x1, waiting for transfers between devices, exchange(): lax.all_to_all(x, PART, split_axis=0, concat_axis=0, axis_index_groups=me...  3.83 us
    all_to_all x1, starting transfers between devices, exchange(): lax.all_to_all(x, PART, split_axis=0, concat_axis=0, axis_index_groups=me...  3.54 us
    pallas_call x1, Pallas kernels, attend(): pl.pallas_call(functools.partial(attend_kernel, heads, sizes), out_shape=...  3.39 us
    pallas_call x1, Pallas kernels, piece_queries(): pl.pallas_call(functools.partial(proj_kernel, heads), out_shape=jax.Shape...  3.35 us
    ppermute x1, starting transfers between devices, swapped(): return lax.ppermute(x, 'tp', [(0, 1), (1, 0)])  2.95 us
  transfers between devices with their start and end apart: 2, of which 2 were waited for; matrix products, arithmetic and copies ran while one was open for 1% of the time, Pallas kernels for 8%

profile of v1, /device:TPU:1, one launch (start us, length us, event | category | flops | bytes accessed | tf_op | source)
XLA Modules:
  0.0 75.7 jit_solution(4884989593490610675)
XLA Ops:
  0.6 0.0 copy-start.4
  0.6 0.0 copy-start.3
  0.7 0.0 copy-start.5
  0.7 0.0 copy-start.6
  0.7 0.0 copy-start.1
  0.7 0.0 copy-start.2
  0.7 0.0 copy-start.8
  0.7 3.4 %piece_queries.1 = bf16[16,72,128]{2,1,0:T(8,128)(2,1)} custom-call(bf16[16,2048]{1,0:T(8,128)(2,1)} %tok_ref.1, f32[1,2048]{1,0:T(1,128)} %bitcast.8, bf16[2048,512]{1,0:T(8,128)(2,1)} %wq_hbm.3, bf16[4,2048]{1,0:T(4,128)(2,1)} %bitcast.16, f32[1,4]{1,0:T(1,128)} %bitcast.18), custom_call_target="tpu_custom_call" | custom-call | flops 45000000 | bytes 2097152 | tf_op jit(solution)/shard_map/piece_queries/pallas_call | solution.py:134
  4.1 28.1 %all_to_all.15.shared_ref = bf16[16,72,128]{2,1,0:T(8,128)(2,1)S(1)} all-to-all(bf16[16,72,128]{2,1,0:T(8,128)(2,1)} %piece_queries.1), channel_id=1, replica_groups={{0,2,4,6,8,10,12,14,16,18,20,22,24,26,28,30},{1,3,17,19,33,35,49,51,65,..., dimensions={0} | all-to-all | bytes 589824 | tf_op jit(solution)/shard_map/all_to_all | solution.py:661
  32.2 0.0 copy-done.4
  32.2 0.0 copy-done.3
  32.2 0.0 copy-done.5
  32.2 0.0 copy-done.6
  32.2 0.0 copy-done.1
  32.2 0.0 copy-done.2
  32.2 0.0 copy-done.8
  32.2 0.3 block_payload.1
  32.6 19.6 %all_to_all.16.new_ref = bf16[4,592,128]{2,1,0:T(8,128)(2,1)S(1)} all-to-all(bf16[4,592,128]{2,1,0:T(8,128)(2,1)S(1)} %block_payload.1), channel_id=1, replica_groups={{0,32,64,96},{1,5,9,13},{2,34,66,98},{3,7,11,15},{4,36,68,100},{6,38,70..., dimensions={0} | all-to-all | bytes 1212416 | tf_op jit(solution)/shard_map/all_to_all | solution.py:661
  52.2 3.4 %attend.1 = bf16[16,72,128]{2,1,0:T(8,128)(2,1)} custom-call(bf16[16,72,128]{2,1,0:T(8,128)(2,1)S(1)} %all_to_all.15.shared_ref, bf16[4,592,128]{2,1,0:T(8,128)(2,1)S(1)} %all_to_all.16.new_ref), custom_call_target="tpu_custom_call" | custom-call | flops 60000000 | bytes 1048576 | tf_op jit(solution)/shard_map/attend/pallas_call | solution.py:359
  55.5 3.5 %all-to-all-start.2 = ((bf16[16,72,128]{2,1,0:T(8,128)(2,1)}), bf16[16,72,128]{2,1,0:T(8,128)(2,1)S(1)}, u32[]{:S(2)}, u32[]{:S(2)}) async-start(bf16[16,72,128]{2,1,0:T(8,128)(2,1)} %attend.1), calls=%async_computation.2 | async-start | bytes 589824 | tf_op jit(solution)/shard_map/all_to_all | solution.py:661
  59.1 0.0 copy-start
  59.1 6.0 %decode.1 = bf16[48,2048]{1,0:T(8,128)(2,1)} custom-call(s32[12]{0:T(128)} %lengths_ref.1, bf16[12,4,2048]{2,1,0:T(4,128)(2,1)} %tok_hbm.3, f32[1,2048]{1,0:T(1,128)} %bitcast.9, bf16[2048,512]{1,0:T(8,128)(2,1)} %wq_hbm.3, bf16[2048,128]{1,0:T(8,128)(2,1)} %wk_hbm.1, bf16[2048,128]{1,0:T(8,128)(2,1)} %wv_hbm.1, bf16[4,2048]{1,0:T(4,128)(2,1)} %bitcast.17, ...), custom_call_target="tpu_custom_call" | custom-call | flops 90000000 | bytes 8388608 | tf_op jit(solution)/shard_map/decode/pallas_call | solution.py:591
  65.1 0.0 copy-start.7
  65.1 1.0 %pad.4.dec_ref = bf16[64,2048]{1,0:T(8,128)(2,1)S(1)} pad(bf16[48,2048]{1,0:T(8,128)(2,1)} %decode.1, bf16[]{:T(256)} %constant.2.clone.1), padding=16_0x0_0 | pad | bytes 458754 | tf_op jit(solution)/shard_map/jit(_pad)/pad | solution.py:726
  66.1 3.8 %all-to-all-done.2.back_ref = bf16[16,72,128]{2,1,0:T(8,128)(2,1)S(1)} async-done(((bf16[16,72,128]{2,1,0:T(8,128)(2,1)}), bf16[16,72,128]{2,1,0:T(8,128)(2,1)S(1)}, u32[]{:S(2)}, u32[]{:S(2)}) %all-to-all-start.2) | async-done | bytes 294944 | tf_op jit(solution)/shard_map/all_to_all | solution.py:661
  69.9 0.0 copy-done
  69.9 0.8 %merge.1.one_ref = bf16[64,2048]{1,0:T(8,128)(2,1)S(1)} custom-call(bf16[16,72,128]{2,1,0:T(8,128)(2,1)S(1)} %all-to-all-done.2.back_ref, bf16[512,2048]{1,0:T(8,128)(2,1)S(1)} %copy-done, bf16[64,2048]{1,0:T(8,128)(2,1)S(1)} %pad.4.dec_ref), custom_call_target="tpu_custom_call" | custom-call | flops 30000000 | bytes 2097152 | tf_op jit(solution)/shard_map/merge/pallas_call | solution.py:403
  70.7 2.9 %collective-permute-start = (bf16[64,2048]{1,0:T(8,128)(2,1)S(1)}, bf16[64,2048]{1,0:T(8,128)(2,1)S(1)}, u32[]{:S(2)}, u32[]{:S(2)}) collective-permute-start(bf16[64,2048]{1,0:T(8,128)(2,1)S(1)} %merge.1.one_ref), channel_id=1, source_target_pairs={{0,1},{1,0},{2,3},{3,2},{4,5},{5,4},{6,7},{7,6},{8,9},{9,8},{10,11... | collective-permute-start | bytes 786440 | tf_op jit(solution)/shard_map/ppermute | solution.py:667
  73.6 1.1 %collective-permute-done.two_ref = bf16[64,2048]{1,0:T(8,128)(2,1)S(1)} collective-permute-done((bf16[64,2048]{1,0:T(8,128)(2,1)S(1)}, bf16[64,2048]{1,0:T(8,128)(2,1)S(1)}, u32[]{:S(2)}, u32[]{:S(2)}) %collective-permute-start) | collective-permute-done | bytes 262176 | tf_op jit(solution)/shard_map/ppermute | solution.py:667
  74.8 0.0 copy-done.7
  74.8 0.9 %final.1 = (bf16[16,2048]{1,0:T(8,128)(2,1)}, bf16[12,4,2048]{2,1,0:T(4,128)(2,1)}) custom-call(bf16[64,2048]{1,0:T(8,128)(2,1)S(1)} %merge.1.one_ref, bf16[64,2048]{1,0:T(8,128)(2,1)S(1)} %collective-permute-done.two_ref, f32[1,2048]{1,0:T(1,128)S(1)} %bitcast.13), custom_call_target="tpu_custom_call" | custom-call | flops 7500000 | bytes 131072 | tf_op jit(solution)/shard_map/final/pallas_call | solution.py:428
Async XLA Ops:
  0.6 31.5 %copy-start.4 = (f32[2048]{0:T(1024)S(1)}, f32[2048]{0:T(1024)}, u32[]{:S(2)}) copy-start(f32[2048]{0:T(1024)} %param.19) | copy-start | bytes 24580
  0.6 31.5 %copy-start.3 = (bf16[16,2048]{1,0:T(8,128)(2,1)S(1)}, bf16[16,2048]{1,0:T(8,128)(2,1)}, u32[]{:S(2)}) copy-start(bf16[16,2048]{1,0:T(8,128)(2,1)} %tok_ref.1) | copy-start | bytes 196612
  0.7 31.5 %copy-start.5 = (bf16[256,1,128]{2,0,1:T(8,128)(2,1)S(1)}, bf16[256,1,128]{2,0,1:T(8,128)(2,1)}, u32[]{:S(2)}) copy-start(bf16[256,1,128]{2,0,1:T(8,128)(2,1)} %param.27) | copy-start | bytes 196612
  0.7 31.5 %copy-start.6 = (bf16[256,1,128]{2,0,1:T(8,128)(2,1)S(1)}, bf16[256,1,128]{2,0,1:T(8,128)(2,1)}, u32[]{:S(2)}) copy-start(bf16[256,1,128]{2,0,1:T(8,128)(2,1)} %param.28) | copy-start | bytes 196612
  0.7 31.5 %copy-start.1 = (bf16[2048,128]{1,0:T(8,128)(2,1)S(1)}, bf16[2048,128]{1,0:T(8,128)(2,1)}, u32[]{:S(2)}) copy-start(bf16[2048,128]{1,0:T(8,128)(2,1)} %wk_hbm.1) | copy-start | bytes 1572868
  0.7 31.5 %copy-start.2 = (bf16[2048,128]{1,0:T(8,128)(2,1)S(1)}, bf16[2048,128]{1,0:T(8,128)(2,1)}, u32[]{:S(2)}) copy-start(bf16[2048,128]{1,0:T(8,128)(2,1)} %wv_hbm.1) | copy-start | bytes 1572868
  0.7 31.5 %copy-start.8 = (f32[4,256]{1,0:T(4,128)S(1)}, f32[4,256]{1,0:T(4,128)}, u32[]{:S(2)}) copy-start(f32[4,256]{1,0:T(4,128)} %gate_ref.1) | copy-start | bytes 12292
  55.5 14.3 %all-to-all-start.2 = ((bf16[16,72,128]{2,1,0:T(8,128)(2,1)}), bf16[16,72,128]{2,1,0:T(8,128)(2,1)S(1)}, u32[]{:S(2)}, u32[]{:S(2)}) async-start(bf16[16,72,128]{2,1,0:T(8,128)(2,1)} %attend.1), calls=%async_computation.2 | async-start | bytes 589824 | tf_op jit(solution)/shard_map/all_to_all | solution.py:661
  59.1 10.8 %copy-start = (bf16[512,2048]{1,0:T(8,128)(2,1)S(1)}, bf16[512,2048]{1,0:T(8,128)(2,1)}, u32[]{:S(2)}) copy-start(bf16[512,2048]{1,0:T(8,128)(2,1)} %wo_ref.1) | copy-start | bytes 6291460
  65.1 9.7 %copy-start.7 = (f32[2048]{0:T(1024)S(1)}, f32[2048]{0:T(1024)}, u32[]{:S(2)}) copy-start(f32[2048]{0:T(1024)} %param.26) | copy-start | bytes 24580
  70.7 4.1 %collective-permute-start = (bf16[64,2048]{1,0:T(8,128)(2,1)S(1)}, bf16[64,2048]{1,0:T(8,128)(2,1)S(1)}, u32[]{:S(2)}, u32[]{:S(2)}) collective-permute-start(bf16[64,2048]{1,0:T(8,128)(2,1)S(1)} %merge.1.one_ref), channel_id=1, source_target_pairs={{0,1},{1,0},{2,3},{3,2},{4,5},{5,4},{6,7},{7,6},{8,9},{9,8},{10,11... | collective-permute-start | bytes 786440 | tf_op jit(solution)/shard_map/ppermute | solution.py:667

commit v2 on v1

--- a/solution.py
+++ b/solution.py
@@ -79,12 +79,29 @@
 
 
 def proj_kernel(
-    heads, tok_hbm, gain_ref, wq_hbm, wg_ref, bias_ref, share_ref, tok_ref, wq_ref, sems
+    heads,
+    tok_hbm,
+    gain_hbm,
+    wq_hbm,
+    wg_hbm,
+    bias_hbm,
+    share_ref,
+    tok_ref,
+    gain_ref,
+    wq_ref,
+    wg_ref,
+    bias_ref,
+    sems,
 ):
     model, width = wq_ref.shape
-    pieces = sems.shape[0] - 1
+    pieces = sems.shape[0] - 4
     depth = model // pieces
-    moves = [(tok_hbm, tok_ref)]
+    moves = [
+        (tok_hbm, tok_ref),
+        (gain_hbm, gain_ref),
+        (wg_hbm, wg_ref),
+        (bias_hbm, bias_ref),
+    ]
     moves += [
         (wq_hbm.at[pl.ds(n * depth, depth)], wq_ref.at[pl.ds(n * depth, depth)])
         for n in range(pieces)
@@ -92,7 +109,8 @@
     copies = [pltpu.make_async_copy(src, dst, sems.at[n]) for n, (src, dst) in enumerate(moves)]
     for copy in copies:
         copy.start()
-    copies[0].wait()
+    for copy in copies[0:4]:
+        copy.wait()
     normed = rms_scale(tok_ref[...], gain_ref[...]).astype(BF16)
     rows = normed.shape[0]
     logits = dot_t(normed, wg_ref[...]) + bias_ref[...]
@@ -109,7 +127,7 @@
     packed = fold_rows(pack_lanes(run, heads)).astype(BF16)
     queries = jnp.zeros((rows, width), F32)
     for n in range(pieces):
-        copies[1 + n].wait()
+        copies[4 + n].wait()
         queries = queries + jnp.dot(
             normed[:, n * depth : (n + 1) * depth],
             wq_ref[n * depth : (n + 1) * depth, :],
@@ -136,12 +154,15 @@
         out_shape=jax.ShapeDtypeStruct(
             (near, heads * rows + rows // 2, width // heads), BF16
         ),
-        in_specs=[hbm, vmem, hbm, vmem, vmem],
+        in_specs=[hbm] * 5,
         out_specs=vmem,
         scratch_shapes=[
             pltpu.VMEM((rows, model), BF16),
+            pltpu.VMEM((1, model), F32),
             pltpu.VMEM((model, width), BF16),
-            pltpu.SemaphoreType.DMA((5,)),
+            pltpu.VMEM((heads, model), BF16),
+            pltpu.VMEM((1, heads), F32),
+            pltpu.SemaphoreType.DMA((8,)),
         ],
         cost_estimate=cost(3.0, 2 << 20),
         name="piece_queries",

time: 76.1 us -> 75.4 us (level)
  no operation moved by 1% of the time
where the time goes in v2:
time: 75.4 us; the launch traced here: 75 us
  blocking collectives  47.7 us (63%)
  Pallas kernels  14.1 us (19%)
  starting transfers between devices  6.49 us (9%)
  waiting for transfers between devices  4.97 us (7%)
  local copies, waits for them, and re-layouts  1 us (1%)
  between operations  0.78 us (1%)
    all_to_all x2, blocking collectives, exchange(): lax.all_to_all(x, PART, split_axis=0, concat_axis=0, axis_index_groups=me...  47.7 us
    pallas_call x1, Pallas kernels, decode(): pl.pallas_call(dec_kernel, out_shape=jax.ShapeDtypeStruct((seqs * new, wo...  5.97 us
    all_to_all x1, waiting for transfers between devices, exchange(): lax.all_to_all(x, PART, split_axis=0, concat_axis=0, axis_index_groups=me...  3.83 us
    all_to_all x1, starting transfers between devices, exchange(): lax.all_to_all(x, PART, split_axis=0, concat_axis=0, axis_index_groups=me...  3.54 us
    pallas_call x1, Pallas kernels, attend(): pl.pallas_call(functools.partial(attend_kernel, heads, sizes), out_shape=...  3.39 us
    ppermute x1, starting transfers between devices, swapped(): return lax.ppermute(x, 'tp', [(0, 1), (1, 0)])  2.95 us
    pallas_call x1, Pallas kernels, piece_queries(): pl.pallas_call(functools.partial(proj_kernel, heads), out_shape=jax.Shape...  2.67 us
  transfers between devices with their start and end apart: 2, of which 2 were waited for; matrix products, arithmetic and copies ran while one was open for 1% of the time, Pallas kernels for 8%

profile of v2, /device:TPU:1, one launch (start us, length us, event | category | flops | bytes accessed | tf_op | source)
XLA Modules:
  0.0 75.0 jit_solution(4638081040490761782)
XLA Ops:
  0.6 0.0 copy-start.4
  0.6 0.0 copy-start.3
  0.7 0.0 copy-start.5
  0.7 0.0 copy-start.6
  0.7 0.0 copy-start.1
  0.7 0.0 copy-start.2
  0.7 0.0 copy-start.8
  0.7 2.7 %piece_queries.1 = bf16[16,72,128]{2,1,0:T(8,128)(2,1)} custom-call(bf16[16,2048]{1,0:T(8,128)(2,1)} %tok_ref.1, f32[1,2048]{1,0:T(1,128)} %bitcast.8, bf16[2048,512]{1,0:T(8,128)(2,1)} %wq_hbm.3, bf16[4,2048]{1,0:T(4,128)(2,1)} %bitcast.16, f32[1,4]{1,0:T(1,128)} %bitcast.18), custom_call_target="tpu_custom_call" | custom-call | flops 45000000 | bytes 2097152 | tf_op jit(solution)/shard_map/piece_queries/pallas_call | solution.py:152
  3.4 28.1 %all_to_all.15.shared_ref = bf16[16,72,128]{2,1,0:T(8,128)(2,1)S(1)} all-to-all(bf16[16,72,128]{2,1,0:T(8,128)(2,1)} %piece_queries.1), channel_id=1, replica_groups={{0,2,4,6,8,10,12,14,16,18,20,22,24,26,28,30},{1,3,17,19,33,35,49,51,65,..., dimensions={0} | all-to-all | bytes 589824 | tf_op jit(solution)/shard_map/all_to_all | solution.py:682
  31.5 0.0 copy-done.4
  31.5 0.0 copy-done.3
  31.5 0.0 copy-done.5
  31.5 0.0 copy-done.6
  31.5 0.0 copy-done.1
  31.5 0.0 copy-done.2
  31.5 0.0 copy-done.8
  31.5 0.3 block_payload.1
  31.9 19.6 %all_to_all.16.new_ref = bf16[4,592,128]{2,1,0:T(8,128)(2,1)S(1)} all-to-all(bf16[4,592,128]{2,1,0:T(8,128)(2,1)S(1)} %block_payload.1), channel_id=1, replica_groups={{0,32,64,96},{1,5,9,13},{2,34,66,98},{3,7,11,15},{4,36,68,100},{6,38,70..., dimensions={0} | all-to-all | bytes 1212416 | tf_op jit(solution)/shard_map/all_to_all | solution.py:682
  51.5 3.4 %attend.1 = bf16[16,72,128]{2,1,0:T(8,128)(2,1)} custom-call(bf16[16,72,128]{2,1,0:T(8,128)(2,1)S(1)} %all_to_all.15.shared_ref, bf16[4,592,128]{2,1,0:T(8,128)(2,1)S(1)} %all_to_all.16.new_ref), custom_call_target="tpu_custom_call" | custom-call | flops 60000000 | bytes 1048576 | tf_op jit(solution)/shard_map/attend/pallas_call | solution.py:380
  54.9 3.5 %all-to-all-start.2 = ((bf16[16,72,128]{2,1,0:T(8,128)(2,1)}), bf16[16,72,128]{2,1,0:T(8,128)(2,1)S(1)}, u32[]{:S(2)}, u32[]{:S(2)}) async-start(bf16[16,72,128]{2,1,0:T(8,128)(2,1)} %attend.1), calls=%async_computation.2 | async-start | bytes 589824 | tf_op jit(solution)/shard_map/all_to_all | solution.py:682
  58.4 0.0 copy-start
  58.4 6.0 %decode.1 = bf16[48,2048]{1,0:T(8,128)(2,1)} custom-call(s32[12]{0:T(128)} %lengths_ref.1, bf16[12,4,2048]{2,1,0:T(4,128)(2,1)} %tok_hbm.3, f32[1,2048]{1,0:T(1,128)} %bitcast.9, bf16[2048,512]{1,0:T(8,128)(2,1)} %wq_hbm.3, bf16[2048,128]{1,0:T(8,128)(2,1)} %wk_hbm.1, bf16[2048,128]{1,0:T(8,128)(2,1)} %wv_hbm.1, bf16[4,2048]{1,0:T(4,128)(2,1)} %bitcast.17, ...), custom_call_target="tpu_custom_call" | custom-call | flops 90000000 | bytes 8388608 | tf_op jit(solution)/shard_map/decode/pallas_call | solution.py:612
  64.4 0.0 copy-start.7
  64.4 1.0 %pad.4.dec_ref = bf16[64,2048]{1,0:T(8,128)(2,1)S(1)} pad(bf16[48,2048]{1,0:T(8,128)(2,1)} %decode.1, bf16[]{:T(256)} %constant.2.clone.1), padding=16_0x0_0 | pad | bytes 458754 | tf_op jit(solution)/shard_map/jit(_pad)/pad | solution.py:747
  65.4 3.8 %all-to-all-done.2.back_ref = bf16[16,72,128]{2,1,0:T(8,128)(2,1)S(1)} async-done(((bf16[16,72,128]{2,1,0:T(8,128)(2,1)}), bf16[16,72,128]{2,1,0:T(8,128)(2,1)S(1)}, u32[]{:S(2)}, u32[]{:S(2)}) %all-to-all-start.2) | async-done | bytes 294944 | tf_op jit(solution)/shard_map/all_to_all | solution.py:682
  69.2 0.0 copy-done
  69.2 0.8 %merge.1.one_ref = bf16[64,2048]{1,0:T(8,128)(2,1)S(1)} custom-call(bf16[16,72,128]{2,1,0:T(8,128)(2,1)S(1)} %all-to-all-done.2.back_ref, bf16[512,2048]{1,0:T(8,128)(2,1)S(1)} %copy-done, bf16[64,2048]{1,0:T(8,128)(2,1)S(1)} %pad.4.dec_ref), custom_call_target="tpu_custom_call" | custom-call | flops 30000000 | bytes 2097152 | tf_op jit(solution)/shard_map/merge/pallas_call | solution.py:424
  70.0 2.9 %collective-permute-start = (bf16[64,2048]{1,0:T(8,128)(2,1)S(1)}, bf16[64,2048]{1,0:T(8,128)(2,1)S(1)}, u32[]{:S(2)}, u32[]{:S(2)}) collective-permute-start(bf16[64,2048]{1,0:T(8,128)(2,1)S(1)} %merge.1.one_ref), channel_id=1, source_target_pairs={{0,1},{1,0},{2,3},{3,2},{4,5},{5,4},{6,7},{7,6},{8,9},{9,8},{10,11... | collective-permute-start | bytes 786440 | tf_op jit(solution)/shard_map/ppermute | solution.py:688
  72.9 1.1 %collective-permute-done.two_ref = bf16[64,2048]{1,0:T(8,128)(2,1)S(1)} collective-permute-done((bf16[64,2048]{1,0:T(8,128)(2,1)S(1)}, bf16[64,2048]{1,0:T(8,128)(2,1)S(1)}, u32[]{:S(2)}, u32[]{:S(2)}) %collective-permute-start) | collective-permute-done | bytes 262176 | tf_op jit(solution)/shard_map/ppermute | solution.py:688
  74.1 0.0 copy-done.7
  74.1 0.9 %final.1 = (bf16[16,2048]{1,0:T(8,128)(2,1)}, bf16[12,4,2048]{2,1,0:T(4,128)(2,1)}) custom-call(bf16[64,2048]{1,0:T(8,128)(2,1)S(1)} %merge.1.one_ref, bf16[64,2048]{1,0:T(8,128)(2,1)S(1)} %collective-permute-done.two_ref, f32[1,2048]{1,0:T(1,128)S(1)} %bitcast.13), custom_call_target="tpu_custom_call" | custom-call | flops 7500000 | bytes 131072 | tf_op jit(solution)/shard_map/final/pallas_call | solution.py:449
Async XLA Ops:
  0.6 30.9 %copy-start.4 = (f32[2048]{0:T(1024)S(1)}, f32[2048]{0:T(1024)}, u32[]{:S(2)}) copy-start(f32[2048]{0:T(1024)} %param.19) | copy-start | bytes 24580
  0.6 30.9 %copy-start.3 = (bf16[16,2048]{1,0:T(8,128)(2,1)S(1)}, bf16[16,2048]{1,0:T(8,128)(2,1)}, u32[]{:S(2)}) copy-start(bf16[16,2048]{1,0:T(8,128)(2,1)} %tok_ref.1) | copy-start | bytes 196612
  0.7 30.8 %copy-start.5 = (bf16[256,1,128]{2,0,1:T(8,128)(2,1)S(1)}, bf16[256,1,128]{2,0,1:T(8,128)(2,1)}, u32[]{:S(2)}) copy-start(bf16[256,1,128]{2,0,1:T(8,128)(2,1)} %param.27) | copy-start | bytes 196612
  0.7 30.8 %copy-start.6 = (bf16[256,1,128]{2,0,1:T(8,128)(2,1)S(1)}, bf16[256,1,128]{2,0,1:T(8,128)(2,1)}, u32[]{:S(2)}) copy-start(bf16[256,1,128]{2,0,1:T(8,128)(2,1)} %param.28) | copy-start | bytes 196612
  0.7 30.8 %copy-start.1 = (bf16[2048,128]{1,0:T(8,128)(2,1)S(1)}, bf16[2048,128]{1,0:T(8,128)(2,1)}, u32[]{:S(2)}) copy-start(bf16[2048,128]{1,0:T(8,128)(2,1)} %wk_hbm.1) | copy-start | bytes 1572868
  0.7 30.8 %copy-start.2 = (bf16[2048,128]{1,0:T(8,128)(2,1)S(1)}, bf16[2048,128]{1,0:T(8,128)(2,1)}, u32[]{:S(2)}) copy-start(bf16[2048,128]{1,0:T(8,128)(2,1)} %wv_hbm.1) | copy-start | bytes 1572868
  0.7 30.8 %copy-start.8 = (f32[4,256]{1,0:T(4,128)S(1)}, f32[4,256]{1,0:T(4,128)}, u32[]{:S(2)}) copy-start(f32[4,256]{1,0:T(4,128)} %gate_ref.1) | copy-start | bytes 12292
  54.9 14.3 %all-to-all-start.2 = ((bf16[16,72,128]{2,1,0:T(8,128)(2,1)}), bf16[16,72,128]{2,1,0:T(8,128)(2,1)S(1)}, u32[]{:S(2)}, u32[]{:S(2)}) async-start(bf16[16,72,128]{2,1,0:T(8,128)(2,1)} %attend.1), calls=%async_computation.2 | async-start | bytes 589824 | tf_op jit(solution)/shard_map/all_to_all | solution.py:682
  58.4 10.8 %copy-start = (bf16[512,2048]{1,0:T(8,128)(2,1)S(1)}, bf16[512,2048]{1,0:T(8,128)(2,1)}, u32[]{:S(2)}) copy-start(bf16[512,2048]{1,0:T(8,128)(2,1)} %wo_ref.1) | copy-start | bytes 6291460
  64.4 9.7 %copy-start.7 = (f32[2048]{0:T(1024)S(1)}, f32[2048]{0:T(1024)}, u32[]{:S(2)}) copy-start(f32[2048]{0:T(1024)} %param.26) | copy-start | bytes 24580
  70.0 4.1 %collective-permute-start = (bf16[64,2048]{1,0:T(8,128)(2,1)S(1)}, bf16[64,2048]{1,0:T(8,128)(2,1)S(1)}, u32[]{:S(2)}, u32[]{:S(2)}) collective-permute-start(bf16[64,2048]{1,0:T(8,128)(2,1)S(1)} %merge.1.one_ref), channel_id=1, source_target_pairs={{0,1},{1,0},{2,3},{3,2},{4,5},{5,4},{6,7},{7,6},{8,9},{9,8},{10,11... | collective-permute-start | bytes 786440 | tf_op jit(solution)/shard_map/ppermute | solution.py:688
